TPU v7x, 32 devices: a whole 2x2x4 slice. The times are simulated.
32 devices in a mesh: ep: 8 (over z, x), tp: 4 (over y, core).
Axes of the slice: x: 2, y: 2, z: 4, core: 2. Of those that a mesh axis runs over, the one named last changes fastest.
Arguments:
- mix_input: bfloat16 [3072, 2048], P('ep', 'tp'), may hold values from -6 to 6
- mix_gain: float32 [2048], replicated, may hold values from 0.1 to 1.9
- gate_b_weight: bfloat16 [2048, 2048], P(None, 'tp'), may hold values from -0.125 to 0.125
- gate_c_weight: bfloat16 [2048, 2048], P(None, 'tp'), may hold values from -0.125 to 0.125
- value_weight: bfloat16 [2048, 2048], P(None, 'tp'), may hold values from -0.125 to 0.125
- conv_weight: float32 [3, 2048], P(None, 'tp'), may hold values from -3 to 3
- out_weight: bfloat16 [2048, 2048], P('tp'), may hold values from -0.125 to 0.125
- expert_input: bfloat16 [1280, 2048], P('ep', 'tp'), may hold values from -6 to 6
- expert_gain: float32 [2048], replicated, may hold values from 0.1 to 1.9
- routes: int32 [1280, 2], P('ep'), may hold values from 0 to 7, all different within a row; in each aligned block of 160 rows (0 to 159, 160 to 319, ...) at most 80 rows name the same one
- route_weight: float32 [1280, 2], P('ep'), may hold values from 0.2 to 1
- expert_gate: bfloat16 [8, 2048, 3072], P('ep', None, 'tp'), may hold values from -0.125 to 0.125
- expert_up: bfloat16 [8, 2048, 3072], P('ep', None, 'tp'), may hold values from -0.125 to 0.125
- expert_down: bfloat16 [8, 3072, 2048], P('ep', 'tp'), may hold values from -0.109375 to 0.109375
Outputs:
- mix_output: bfloat16 [3072, 2048], P('ep', 'tp')
- expert_output: bfloat16 [1280, 2048], P('ep', 'tp')
Inputs may be any that keep to these rules, and one draw needn't show every extreme that they name: `routes`: the 2 experts of a row differ. Among the rows of one device no expert is named more than 80 times, a bound that some block reaches.
All inputs are finite; a program needn't handle non-finite values.
Results may differ from a plain program's by a relative error of at most 0.019.
Values may be sent and summed in bfloat16 or wider, within the bound.
A program may use at most 64 MiB of HBM per device.

v0:
```python
import jax
import jax.numpy as jnp
from jax import lax
from jax.sharding import PartitionSpec as P

epsilon = 1e-06
routed_scale = 2.5


def passed_along(block, axis, distance):
    devices = range(lax.axis_size(axis))
    route = [(i - distance, i) for i in devices if i - distance in devices]
    return lax.ppermute(block, axis, route)


def project_piece(piece, gain_vector, matrices, group_count):
    widened = piece.astype(jnp.float32)
    columns = piece.shape[-1]
    scaled = (widened * gain_vector).astype(jnp.bfloat16)
    grouped = scaled.reshape(group_count, -1, columns)
    updated = tuple(
        (
            jnp.einsum("gsd,gdf->gsf", grouped, matrix, preferred_element_type=jnp.float32)
            for matrix in matrices
        )
    )
    return (updated, jnp.sum(widened * widened, axis=-1))


def local(
    mix_input,
    mix_gain,
    gate_b_weight,
    gate_c_weight,
    value_weight,
    conv_weight,
    out_weight,
    expert_input,
    expert_gain,
    routes,
    route_weight,
    expert_gate,
    expert_up,
    expert_down,
):
    ep_count = lax.axis_size("ep")
    local_experts = expert_gate.shape[0]
    model_width = mix_gain.shape[0]
    expert_count = local_experts * ep_count
    tok_local, top_count = routes.shape
    capacity = 2 * tok_local * top_count // expert_count
    feature_local = expert_input.shape[1]
    mix_rows = mix_input.shape[0]
    slot_rows = ep_count * capacity
    flat_routes = routes.reshape(-1)
    pair_count = flat_routes.shape[0]
    matches = (
        flat_routes[:, None] == lax.broadcasted_iota(jnp.int32, (pair_count, expert_count), 1)
    ).astype(jnp.int32)
    ranks = jnp.sum((jnp.cumsum(matches, axis=0) - matches) * matches, axis=1)
    slot_iota = lax.broadcasted_iota(jnp.int32, (pair_count, expert_count * capacity), 1)
    send_table = (slot_iota == (flat_routes * capacity + ranks)[:, None]).astype(jnp.bfloat16)
    back_index = (
        flat_routes % local_experts * slot_rows + flat_routes // local_experts * capacity + ranks
    )
    back_table = (slot_iota == back_index[:, None]).astype(jnp.bfloat16)
    repeated = jnp.repeat(expert_input, top_count, axis=0)
    outgoing = lax.dot_general(
        send_table, repeated, (((0,), (0,)), ((), ())), preferred_element_type=jnp.float32
    ).astype(jnp.bfloat16)
    outgoing = outgoing.reshape(ep_count, local_experts, capacity, feature_local)
    arrived = lax.all_to_all(outgoing, "ep", split_axis=0, concat_axis=2, tiled=True)
    arrived = arrived.reshape(local_experts * slot_rows, feature_local)
    mix_weights = (gate_b_weight[None], gate_c_weight[None], value_weight[None])
    expert_weights = (expert_gate, expert_up)
    mix_carry = project_piece(
        lax.all_gather(mix_input, "tp", axis=1, tiled=True), mix_gain, mix_weights, 1
    )
    expert_carry = project_piece(
        lax.all_gather(arrived, "tp", axis=1, tiled=True),
        expert_gain,
        expert_weights,
        local_experts,
    )
    mix_totals, mix_squares = mix_carry
    mix_factor = lax.rsqrt(mix_squares / model_width + epsilon)[:, None]
    outer_gate = mix_totals[0][0] * mix_factor
    product = mix_totals[1][0] * mix_factor * (mix_totals[2][0] * mix_factor)
    edge_rows = passed_along(product[mix_rows - 2 :], "ep", 1)
    padded = jnp.concatenate([edge_rows, product], axis=0)
    convolved = (
        conv_weight[0] * padded[:mix_rows]
        + conv_weight[1] * padded[1 : mix_rows + 1]
        + conv_weight[2] * padded[2:]
    )
    gated = (outer_gate * convolved).astype(jnp.bfloat16)
    expert_totals, expert_squares = expert_carry
    expert_factor = lax.rsqrt(expert_squares / model_width + epsilon).reshape(
        local_experts, slot_rows, 1
    )
    activated = (
        jax.nn.silu(expert_totals[0] * expert_factor) * (expert_totals[1] * expert_factor)
    ).astype(jnp.bfloat16)
    sliced = out_weight
    mix_sum = lax.psum_scatter(
        lax.dot_general(
            sliced, gated, (((0,), (1,)), ((), ())), preferred_element_type=jnp.float32
        ).astype(jnp.bfloat16),
        "tp",
        scatter_dimension=0,
        tiled=True,
    ).astype(jnp.float32)
    sliced = expert_down
    summed = jnp.einsum("gsf,gfd->dgs", activated, sliced, preferred_element_type=jnp.float32)
    expert_sum = lax.psum_scatter(
        summed.reshape(lax.axis_size("tp") * feature_local, local_experts * slot_rows).astype(
            jnp.bfloat16
        ),
        "tp",
        scatter_dimension=0,
        tiled=True,
    )
    mix_output = mix_sum.T.astype(jnp.bfloat16)
    returning = expert_sum.reshape(feature_local, local_experts, ep_count, capacity)
    returned = lax.all_to_all(returning, "ep", split_axis=2, concat_axis=2, tiled=True)
    returned = returned.reshape(feature_local, local_experts * slot_rows)
    picked = lax.dot_general(
        returned, back_table, (((1,), (1,)), ((), ())), preferred_element_type=jnp.float32
    ).reshape(feature_local, tok_local, top_count)
    normalized = route_weight / jnp.sum(route_weight, axis=1, keepdims=True) * routed_scale
    expert_output = jnp.sum(picked * normalized[None], axis=2).T.astype(jnp.bfloat16)
    return (mix_output, expert_output)


def solution(mesh):
    in_specs = (
        P("ep", "tp"),
        P(),
        P(None, "tp"),
        P(None, "tp"),
        P(None, "tp"),
        P(None, "tp"),
        P("tp", None),
        P("ep", "tp"),
        P(),
        P("ep", None),
        P("ep", None),
        P("ep", None, "tp"),
        P("ep", None, "tp"),
        P("ep", "tp", None),
    )
    out_specs = (P("ep", "tp"), P("ep", "tp"))
    return jax.shard_map(local, mesh=mesh, in_specs=in_specs, out_specs=out_specs, check_vma=False)
```

profile of v0, /device:TPU:0, one launch (start us, length us, event | category | flops | bytes accessed | tf_op | source)
XLA Modules:
  0.0 158.1 jit_solution(9475336010663980682)
XLA Ops:
  7.2 0.9 copy.20
  8.3 0.9 reduce-window.6
  9.6 1.1 broadcast_in_dim.2
  10.7 0.8 reshape.158
  11.5 1.6 %convolution_convert_fusion.2 = bf16[640,512]{1,0:T(8,128)(2,1)S(1)} fusion(bf16[320,512]{1,0:T(8,128)(2,1)} %reshape.158, s32[320]{0:T(512)S(1)} %multiply_add_fusion), kind=kOutput, calls=%fused_computation.18 | convolution fusion | flops 210247680 | bytes 984320 | tf_op jit(solution)/shard_map/dot_general | solution.py:68
  13.1 24.9 %all_to_all.14 = bf16[8,1,80,512]{3,2,1,0:T(8,128)(2,1)} all-to-all(bf16[8,1,80,512]{3,2,1,0:T(8,128)(2,1)S(1)} %bitcast.51), channel_id=1, replica_groups=mesh['ep'=8,'tp'=4] {'ep'}, dimensions={0} | all-to-all | bytes 1310720 | tf_op jit(solution)/shard_map/all_to_all | solution.py:72
  38.1 0.7 all-gather.3.cloned.1.call-update
  38.8 23.6 %all-gather.5.cloned.1.call-done = bf16[640,2048]{1,0:T(8,128)(2,1)} async-done(((bf16[640,512]{1,0:T(8,128)(2,1)}), bf16[640,2048]{1,0:T(8,128)(2,1)}) %all-gather.5.cloned.1.call-update) | async-done | bytes 2621456 | tf_op jit(solution)/shard_map/all_gather | solution.py:80
  62.4 2.5 %fusion.1 = f32[640]{0:T(1024)S(1)} fusion(bf16[640,2048]{1,0:T(8,128)(2,1)} %all-gather.5.cloned.1.call-done), kind=kLoop, calls=%fused_computation.3 | loop fusion | flops 3931520 | bytes 2624000 | tf_op jit(solution)/shard_map/reduce_sum | solution.py:27
  64.9 5.4 %fusion.5 = f32[640,768]{1,0:T(8,128)} fusion(bf16[1,2048,768]{2,1,0:T(8,128)(2,1)} %param.26, bf16[640,2048]{1,0:T(8,128)(2,1)S(1)} %copy-done.1, f32[2048]{0:T(1024)S(1)} %copy-done.7), kind=kOutput, calls=%fused_computation.10 | convolution fusion | flops 2017198080 | bytes 7741440 | tf_op jit(solution)/shard_map/gsd,gdf->gsf/dot_general | solution.py:23
  70.4 10.0 %fusion.9 = bf16[2048,640]{0,1:T(8,128)(2,1)} fusion(bf16[1,768,2048]{2,1,0:T(8,128)(2,1)S(1)} %copy-done, f32[640,768]{1,0:T(8,128)} %fusion.5, bf16[1,2048,768]{2,1,0:T(8,128)(2,1)} %param.25, bf16[640,2048]{1,0:T(8,128)(2,1)} %all-gather.5.cloned.1.call-done, f32[2048]{0:T(1024)S(1)} %copy-done.7, f32[640]{0:T(1024)S(1)} %add_rsqrt_fusion), kind=kOutput, calls=%fused_computation.14 | convolution fusion | flops 4035706880 | bytes 13511168 | tf_op jit(solution)/shard_map/gsf,gfd->dgs/dot_general | solution.py:114
  80.4 3.2 %all-gather.3.cloned.1.call-done = bf16[384,2048]{1,0:T(8,128)(2,1)} async-done(((bf16[384,512]{1,0:T(8,128)(2,1)}), bf16[384,2048]{1,0:T(8,128)(2,1)}) %all-gather.3.cloned.1.call-update) | async-done | bytes 1572880 | tf_op jit(solution)/shard_map/all_gather | solution.py:77
  83.6 1.8 %fusion.3 = f32[384]{0:T(512)S(1)} fusion(bf16[384,2048]{1,0:T(8,128)(2,1)} %all-gather.3.cloned.1.call-done), kind=kLoop, calls=%fused_computation.8 | loop fusion | flops 2358912 | bytes 1574400 | tf_op jit(solution)/shard_map/reduce_sum | solution.py:27
  85.5 3.2 %convolution_multiply_fusion = f32[384,512]{1,0:T(8,128)S(1)} fusion(bf16[2048,512]{1,0:T(8,128)(2,1)} %param.18, bf16[384,2048]{1,0:T(8,128)(2,1)} %all-gather.3.cloned.1.call-done, f32[2048]{0:T(1024)S(1)} %copy-done.8, f32[384]{0:T(512)S(1)} %add_rsqrt_fusion.1), kind=kOutput, calls=%fused_computation.19 | convolution fusion | flops 807862272 | bytes 4466176 | tf_op jit(solution)/shard_map/gsd,gdf->gsf/dot_general | solution.py:23
  88.7 1.0 fusion.19
  89.7 3.4 %collective-permute-start = (f32[2,512]{1,0:T(2,128)S(1)}, f32[2,512]{1,0:T(2,128)S(1)}, u32[]{:S(2)}, u32[]{:S(2)}) collective-permute-start(f32[2,512]{1,0:T(2,128)S(1)} %slice.36), channel_id=1, source_target_pairs={{0,4},{4,8},{8,12},{12,16},{16,20},{20,24},{24,28},{1,5},{5,9},{9,... | collective-permute-start | bytes 12296 | tf_op jit(solution)/shard_map/ppermute | solution.py:13
  93.1 1.3 collective-permute-done
  94.4 6.7 %fusion.12 = bf16[2048,384]{0,1:T(8,128)(2,1)} fusion(bf16[512,2048]{1,0:T(8,128)(2,1)} %param.20, f32[2,512]{1,0:T(2,128)S(1)} %collective-permute-done, f32[384,512]{1,0:T(8,128)} %copy-done.5, bf16[2048,512]{1,0:T(8,128)(2,1)} %param.16, bf16[384,2048]{1,0:T(8,128)(2,1)} %all-gather.3.cloned.1.call-done, f32[2048]{0:T(1024)S(1)} %copy-done.8, ...), kind=kOutput, calls=%fused_computation.16 | convolution fusion | flops 1615724544 | bytes 8146432 | tf_op jit(solution)/shard_map/dot_general | solution.py:106
  101.2 19.4 %reduce-scatter.5.cloned.1.call-done = bf16[512,640]{0,1:T(8,128)(2,1)} async-done(((bf16[2048,640]{0,1:T(8,128)(2,1)}), bf16[512,640]{0,1:T(8,128)(2,1)}) %reduce-scatter.5.cloned.1.call-update) | async-done | bytes 655376 | tf_op jit(solution)/shard_map/reduce_scatter | solution.py:115
  120.6 5.5 %all-to-all-start.1 = ((bf16[512,1,8,80]{0,3,1,2:T(8,128)(2,1)}), bf16[512,1,8,80]{0,3,1,2:T(8,128)(2,1)}, u32[]{:S(2)}, u32[]{:S(2)}) async-start(bf16[512,1,8,80]{0,3,1,2:T(8,128)(2,1)} %bitcast.50), calls=%async_computation.3 | async-start | bytes 1310720 | tf_op jit(solution)/shard_map/all_to_all | solution.py:125
  126.3 1.0 eq.43
  127.3 16.0 %all-to-all-done.1 = bf16[512,1,8,80]{0,3,1,2:T(8,128)(2,1)} async-done(((bf16[512,1,8,80]{0,3,1,2:T(8,128)(2,1)}), bf16[512,1,8,80]{0,3,1,2:T(8,128)(2,1)}, u32[]{:S(2)}, u32[]{:S(2)}) %all-to-all-start.1) | async-done | bytes 655392 | tf_op jit(solution)/shard_map/all_to_all | solution.py:125
  143.3 2.3 %fusion.20 = bf16[512,160]{0,1:T(8,128)(2,1)} fusion(bf16[512,640,1]{0,1,2:T(8,128)(2,1)} %bitcast.18, pred[160,2,640]{2,1,0:T(4,128)(4,1)} %eq.43, f32[160,2]{0,1:T(2,128)S(1)} %divide_multiply_fusion), kind=kOutput, calls=%fused_computation.24 | convolution fusion | flops 209960960 | bytes 1025280 | tf_op jit(solution)/shard_map/dot_general | solution.py:127
  145.7 5.9 %reduce-scatter.3.cloned.1.call-done = bf16[512,384]{0,1:T(8,128)(2,1)} async-done(((bf16[2048,384]{0,1:T(8,128)(2,1)}), bf16[512,384]{0,1:T(8,128)(2,1)}) %reduce-scatter.3.cloned.1.call-update) | async-done | bytes 393232 | tf_op jit(solution)/shard_map/reduce_scatter | solution.py:105
  (40 shorter events, 1.0 us)
Async XLA Ops:
  7.2 63.2 %copy-start = (bf16[1,768,2048]{2,1,0:T(8,128)(2,1)S(1)}, bf16[1,768,2048]{2,1,0:T(8,128)(2,1)}, u32[]{:S(2)}) copy-start(bf16[1,768,2048]{2,1,0:T(8,128)(2,1)} %param.27) | copy-start | bytes 9437188
  7.2 55.2 %all-gather.5.cloned.1.call-start = ((), (), s32[]{:S(2)}) async-start(), calls=%async_computation.6 | async-start | bytes 3276800 | tf_op jit(solution)/shard_map/all_gather | solution.py:80
  38.0 26.9 %copy-start.7 = (f32[2048]{0:T(1024)S(1)}, f32[2048]{0:T(1024)}, u32[]{:S(2)}) copy-start(f32[2048]{0:T(1024)} %param.22) | copy-start | bytes 24580
  38.0 45.6 %all-gather.3.cloned.1.call-start = ((), (), s32[]{:S(2)}) async-start(), calls=%async_computation.4 | async-start | bytes 1966080 | tf_op jit(solution)/shard_map/all_gather | solution.py:77
  38.8 81.8 %reduce-scatter.5.cloned.1.call-start = ((), (), s32[]{:S(2)}) async-start(), calls=%async_computation.7 | async-start | bytes 3276800 | tf_op jit(solution)/shard_map/reduce_scatter | solution.py:115
  62.4 2.5 %copy-start.1 = (bf16[640,2048]{1,0:T(8,128)(2,1)S(1)}, bf16[640,2048]{1,0:T(8,128)(2,1)}, u32[]{:S(2)}) copy-start(bf16[640,2048]{1,0:T(8,128)(2,1)} %all-gather.5.cloned.1.call-done) | copy-start | bytes 7864324
  80.4 5.1 %copy-start.8 = (f32[2048]{0:T(1024)S(1)}, f32[2048]{0:T(1024)}, u32[]{:S(2)}) copy-start(f32[2048]{0:T(1024)} %param.15) | copy-start | bytes 24580
  80.4 71.2 %reduce-scatter.3.cloned.1.call-start = ((), (), s32[]{:S(2)}) async-start(), calls=%async_computation.5 | async-start | bytes 1966080 | tf_op jit(solution)/shard_map/reduce_scatter | solution.py:105
  85.4 3.2 %copy-start.2 = (bf16[384,2048]{1,0:T(8,128)(2,1)S(1)}, bf16[384,2048]{1,0:T(8,128)(2,1)}, u32[]{:S(2)}) copy-start(bf16[384,2048]{1,0:T(8,128)(2,1)} %all-gather.3.cloned.1.call-done) | copy-start | bytes 4718596
  85.4 3.2 %copy-start.6 = (bf16[2048,512]{1,0:T(8,128)(2,1)S(1)}, bf16[2048,512]{1,0:T(8,128)(2,1)}, u32[]{:S(2)}) copy-start(bf16[2048,512]{1,0:T(8,128)(2,1)} %param.17) | copy-start | bytes 6291460
  88.7 4.4 %copy-start.4 = (f32[3,512]{1,0:T(4,128)S(1)}, f32[3,512]{1,0:T(4,128)}, u32[]{:S(2)}) copy-start(f32[3,512]{1,0:T(4,128)} %param.19) | copy-start | bytes 18436
  89.7 4.7 %copy-start.5 = (f32[384,512]{1,0:T(8,128)}, f32[384,512]{1,0:T(8,128)S(1)}, u32[]{:S(2)}) copy-start(f32[384,512]{1,0:T(8,128)S(1)} %fusion.19) | copy-start | bytes 2359300
  89.7 4.7 %collective-permute-start = (f32[2,512]{1,0:T(2,128)S(1)}, f32[2,512]{1,0:T(2,128)S(1)}, u32[]{:S(2)}, u32[]{:S(2)}) collective-permute-start(f32[2,512]{1,0:T(2,128)S(1)} %slice.36), channel_id=1, source_target_pairs={{0,4},{4,8},{8,12},{12,16},{16,20},{20,24},{24,28},{1,5},{5,9},{9,... | collective-permute-start | bytes 12296 | tf_op jit(solution)/shard_map/ppermute | solution.py:13
  101.2 26.1 %copy-start.3 = (f32[160,2]{0,1:T(2,128)S(1)}, f32[160,2]{0,1:T(2,128)}, u32[]{:S(2)}) copy-start(f32[160,2]{0,1:T(2,128)} %param.24) | copy-start | bytes 3844
  120.6 22.7 %all-to-all-start.1 = ((bf16[512,1,8,80]{0,3,1,2:T(8,128)(2,1)}), bf16[512,1,8,80]{0,3,1,2:T(8,128)(2,1)}, u32[]{:S(2)}, u32[]{:S(2)}) async-start(bf16[512,1,8,80]{0,3,1,2:T(8,128)(2,1)} %bitcast.50), calls=%async_computation.3 | async-start | bytes 1310720 | tf_op jit(solution)/shard_map/all_to_all | solution.py:125
Sparse Core Ops, SparseCore 0:
  38.1 24.2 all-gather.4
  64.0 19.6 all-gather.2
  86.2 34.3 reduce-scatter.4
  123.5 27.9 reduce-scatter.2
where the time goes:
time: 158 us
  waiting for transfers between devices  70.1 us (44%)
  matrix products  30.3 us (19%)
  blocking collectives  24.9 us (16%)
  between operations  13.9 us (9%)
  starting transfers between devices  9.05 us (6%)
  other arithmetic  5.51 us (3%)
  local copies, waits for them, and re-layouts  4.3 us (3%)
    all_to_all x1, blocking collectives, local(): lax.all_to_all(outgoing, 'ep', split_axis=0, concat_axis=2, tiled=True)  24.9 us
    all_gather x1, waiting for transfers between devices, local(): lax.all_gather(arrived, 'tp', axis=1, tiled=True)  23.6 us
    reduce_scatter x1, waiting for transfers between devices, local(): lax.psum_scatter(summed.reshape(lax.axis_size('tp') * feature_local, loca...  19.4 us
    all_to_all x1, waiting for transfers between devices, local(): lax.all_to_all(returning, 'ep', split_axis=2, concat_axis=2, tiled=True)  16 us
    dot_general x1, matrix products, local(): jnp.einsum('gsf,gfd->dgs', activated, sliced, preferred_element_type=jnp....  9.98 us
    dot_general x3, matrix products, project_piece(): jnp.einsum('gsd,gdf->gsf', grouped, matrix, preferred_element_type=jnp.fl...  9.62 us
    dot_general x1, matrix products, local(): lax.dot_general(sliced, gated, (((0,), (1,)), ((), ())), preferred_elemen...  6.74 us
    reduce_scatter x1, waiting for transfers between devices, local(): lax.psum_scatter(lax.dot_general(sliced, gated, (((0,), (1,)), ((), ())),...  5.88 us
  transfers between devices with their start and end apart: 6, of which 6 were waited for; matrix products, arithmetic and copies ran while one was open for 22% of the time, Pallas kernels for 0%

commit v1 on v0

v1 whole, which is shorter than its diff:
```python
import functools

import jax
import jax.numpy as jnp
from jax import lax
from jax.experimental import pallas as pl
from jax.experimental.pallas import tpu as pltpu
from jax.sharding import PartitionSpec as P

MESH = pl.DeviceIdType.MESH
epsilon = 1e-06
routed_scale = 2.5
f32 = jnp.float32
bf16 = jnp.bfloat16


def kernel(
    dims,
    mix_ref, mgain_ref, wb_hbm, wc_hbm, wv_hbm, conv_ref, wo_hbm,
    exp_ref, egain_ref, routes_ref, rw_ref, wg_hbm, wu_hbm, wd_hbm,
    mo_ref, eo_ref,
    wb, wc, wv, wo, wg, wu, wd, w_sem,
    tables, outg, xg, xs, fac, outer, prod, edge, gated, pm, rm, sm, ym,
    xe, xes, efac, act, pe, re, se, yr, fin, ret,
    mys, myr, mps, mpr, eps, epr, eys, eyr, pps, ppr, edges,
    rms, rmr, yms, ymr, res, rer, ses, ser, rts, rtr,
):
    n_ep, n_tp, cap, group = dims
    chips = n_tp // 2
    n_group = n_ep // group
    rows, feat = mix_ref.shape
    width = feat * n_tp
    tok = exp_ref.shape[0]
    slots = n_ep * cap
    e = lax.axis_index("ep")
    t = lax.axis_index("tp")
    y, c = lax.div(t, 2), lax.rem(t, 2)
    partner = y * 2 + 1 - c
    home = lax.div(e, group)

    def cols(b):
        return pl.ds(pl.multiple_of(b * feat, feat), feat)

    def remote(src, dst, send_sem, recv_sem, ep, tp):
        return pltpu.make_async_remote_copy(
            src_ref=src, dst_ref=dst, send_sem=send_sem, recv_sem=recv_sem,
            device_id=(ep, tp), device_id_type=MESH,
        )

    def ahead(dy):
        return lax.rem(y + dy, chips) * 2 + c

    def behind(dy):
        return lax.rem(y - dy + chips, chips) * 2 + c

    def loop(count, body):
        lax.fori_loop(0, count, lambda i, carry: (body(i), carry)[1], 0)

    def mix_y(dy):
        return remote(mix_ref, xg.at[:, cols(t)], mys.at[dy], myr.at[dy], e, ahead(dy))

    def mix_p():
        return remote(mix_ref, xg.at[:, cols(t)], mps.at[0], mpr.at[0], e, partner)

    def mix_f(dy):
        part = xg.at[:, cols(behind(dy))]
        return remote(part, part, mps.at[dy], mpr.at[dy], e, partner)

    def dispatch(d):
        s = lax.rem(e + d, n_ep)
        return remote(outg.at[s], xe.at[e, :, cols(t)], eps.at[d], epr.at[d], s, t)

    def span_in(i):
        return pl.ds(lax.rem(home - i + n_group, n_group) * group, group)

    def exp_y(i, dy):
        part = xe.at[span_in(i), :, cols(t)]
        return remote(part, part, eys.at[dy, i], eyr.at[dy, i], e, ahead(dy))

    def exp_p(i):
        part = xe.at[span_in(i), :, cols(t)]
        return remote(part, part, pps.at[0, i], ppr.at[0, i], e, partner)

    def exp_f(i, dy):
        part = xe.at[span_in(i), :, cols(behind(dy))]
        return remote(part, part, pps.at[dy, i], ppr.at[dy, i], e, partner)

    def edge_copy():
        return remote(
            prod.at[pl.ds(rows, 8)], edge, edges.at[0], edges.at[1], lax.rem(e + 1, n_ep), t
        )

    def mix_half(q):
        return remote(pm.at[q * 2 + 1 - c], rm.at[q], rms.at[q], rmr.at[q], e, partner)

    def mix_sum(dy):
        return remote(sm.at[dy], ym.at[dy], yms.at[dy], ymr.at[dy], e, ahead(dy))

    def exp_half(q):
        return remote(pe.at[q * 2 + 1 - c], re.at[q], res.at[q], rer.at[q], e, partner)

    def span_out(i):
        return pl.ds(lax.rem(home + 1 + i, n_group) * group, group)

    def exp_sum(i, dy):
        return remote(
            se.at[dy, span_out(i)], yr.at[dy, span_out(i)],
            ses.at[dy, i], ser.at[dy, i], e, ahead(dy),
        )

    def back(d):
        s = lax.rem(e + d, n_ep)
        return remote(fin.at[s], ret.at[e], rts.at[d], rtr.at[d], s, t)

    loads = [
        pltpu.make_async_copy(src, dst, w_sem.at[i])
        for i, (src, dst) in enumerate(
            ((wb_hbm, wb), (wc_hbm, wc), (wv_hbm, wv), (wo_hbm, wo),
             (wg_hbm, wg), (wu_hbm, wu), (wd_hbm, wd))
        )
    ]
    for load in loads:
        load.start()

    barrier = pltpu.get_barrier_semaphore()
    for dy in range(1, chips):
        pl.semaphore_signal(barrier, inc=1, device_id=(e, ahead(dy)), device_id_type=MESH)
    pl.semaphore_signal(barrier, inc=1, device_id=(e, partner), device_id_type=MESH)

    def greet(d):
        pl.semaphore_signal(
            barrier, inc=1, device_id=(lax.rem(e + d + 1, n_ep), t), device_id_type=MESH
        )

    loop(n_ep - 1, greet)

    lane = lax.broadcasted_iota(jnp.int32, (tok, 128), 1)
    named = [routes_ref[:, k : k + 1] == lane for k in range(2)]
    either = jnp.where(named[0] | named[1], 1.0, 0.0).astype(bf16)
    before = (
        lax.broadcasted_iota(jnp.int32, (tok, tok), 0)
        > lax.broadcasted_iota(jnp.int32, (tok, tok), 1)
    )
    counts = jnp.dot(
        jnp.where(before, 1.0, 0.0).astype(bf16), either, preferred_element_type=f32
    )
    slot_iota = lax.broadcasted_iota(jnp.int32, (tok, slots), 1).astype(f32)
    both = []
    for k in range(2):
        rank = jnp.sum(jnp.where(named[k], counts, 0.0), axis=1, keepdims=True)
        slot = routes_ref[:, k : k + 1].astype(f32) * float(cap) + rank
        one = jnp.where(slot_iota == slot, 1.0, 0.0)
        tables[k] = one.astype(bf16)
        both.append(one)
    send = (both[0] + both[1]).astype(bf16)
    outg[...] = (
        lax.dot_general(
            send, exp_ref[...], (((0,), (0,)), ((), ())), preferred_element_type=f32
        )
        .astype(bf16)
        .reshape(n_ep, cap, feat)
    )

    pl.semaphore_wait(barrier, n_ep - 1 + chips)

    loop(n_ep - 1, lambda d: dispatch(d + 1).start())
    for dy in range(1, chips):
        mix_y(dy).start()
    mix_p().start()
    xe[e, :, cols(t)] = outg[e]
    xg[:, cols(t)] = mix_ref[...]

    def pass_on(i):
        first = lax.rem(home - i + n_group, n_group) * group
        for j in range(group):
            d = lax.rem(e - first - j + n_ep, n_ep)

            @pl.when(d != 0)
            def _():
                dispatch(d).wait_recv()

        for dy in range(1, chips):
            exp_y(i, dy).start()
        exp_p(i).start()

    loop(n_group, pass_on)

    for dy in range(1, chips):
        mix_y(dy).wait_recv()
        mix_f(dy).start()
    mix_p().wait_recv()
    for dy in range(1, chips):
        mix_f(dy).wait_recv()

    tile = 32

    def scale_mix(i):
        at = pl.ds(pl.multiple_of(i * tile, tile), tile)
        x = xg[at].astype(f32)
        fac[at] = lax.rsqrt(jnp.sum(x * x, axis=1, keepdims=True) / width + epsilon)
        xs[at] = (x * mgain_ref[...]).astype(bf16)

    loop(rows // tile, scale_mix)
    for load in loads[:3]:
        load.wait()
    wide = 256 if feat % 256 == 0 else feat

    def project(i):
        at = pl.ds(pl.multiple_of(i * wide, wide), wide)
        x = xs[...]
        factor = fac[...]
        inner = jnp.dot(x, wc[:, at], preferred_element_type=f32) * factor
        values = jnp.dot(x, wv[:, at], preferred_element_type=f32) * factor
        prod[pl.ds(8, rows), at] = inner * values
        outer[:, at] = jnp.dot(x, wb[:, at], preferred_element_type=f32) * factor

    loop(feat // wide, project)
    edge_copy().start()
    edge_copy().wait_recv()
    prod[0:8] = jnp.where(e == 0, 0.0, edge[...])

    def convolve(i):
        at = pl.ds(pl.multiple_of(i * 128, 128), 128)
        convolved = (
            conv_ref[0:1, at] * prod[pl.ds(6, rows), at]
            + conv_ref[1:2, at] * prod[pl.ds(7, rows), at]
            + conv_ref[2:3, at] * prod[pl.ds(8, rows), at]
        )
        gated[:, at] = (outer[:, at] * convolved).astype(bf16)

    loop(feat // 128, convolve)
    loads[3].wait()

    def mix_down(b):
        pm[b] = jnp.dot(gated[...], wo[:, cols(b)], preferred_element_type=f32).astype(bf16)

    loop(n_tp, mix_down)
    for q in range(chips):
        mix_half(q).start()

    def relay(i):
        for dy in range(1, chips):
            exp_y(i, dy).wait_recv()
            exp_f(i, dy).start()

    for q in range(chips):
        mix_half(q).wait_recv()
    for dy in range(1, chips):
        q = lax.rem(y + dy, chips)
        sm[dy] = (pm[ahead(dy)].astype(f32) + rm[q].astype(f32)).astype(bf16)
        mix_sum(dy).start()
    loop(n_group, relay)

    def arrive(i):
        exp_p(i).wait_recv()
        for dy in range(1, chips):
            exp_f(i, dy).wait_recv()

    loop(n_group, arrive)

    def scale_exp(i):
        at = pl.ds(pl.multiple_of(i * cap, cap), cap)
        x = xe[i].astype(f32)
        efac[at] = lax.rsqrt(jnp.sum(x * x, axis=1, keepdims=True) / width + epsilon)
        xes[at] = (x * egain_ref[...]).astype(bf16)

    loop(n_ep, scale_exp)
    loads[4].wait()
    loads[5].wait()
    hidden = wd.shape[0]
    wide_h = 256 if hidden % 256 == 0 else hidden

    def activate(i):
        at = pl.ds(i * wide_h, wide_h) if wide_h == hidden else pl.ds(
            pl.multiple_of(i * wide_h, wide_h), wide_h
        )
        x = xes[...]
        gate = jnp.dot(x, wg[0, :, at], preferred_element_type=f32) * efac[...]
        up = jnp.dot(x, wu[0, :, at], preferred_element_type=f32) * efac[...]
        act[:, at] = (gate / (1.0 + jnp.exp(-gate)) * up).astype(bf16)

    if wide_h == hidden:
        x = xes[...]
        gate = jnp.dot(x, wg[0], preferred_element_type=f32) * efac[...]
        up = jnp.dot(x, wu[0], preferred_element_type=f32) * efac[...]
        act[...] = (gate / (1.0 + jnp.exp(-gate)) * up).astype(bf16)
    else:
        loop(hidden // wide_h, activate)
    loads[6].wait()

    def exp_down(b):
        out = jnp.dot(act[...], wd[:, cols(b)], preferred_element_type=f32)
        pe[b] = out.astype(bf16).reshape(n_ep, cap, feat)

    loop(n_tp, exp_down)
    for q in range(chips):
        exp_half(q).start()

    for q in range(chips):
        exp_half(q).wait_recv()

    def push(i):
        at = span_out(i)
        for dy in range(1, chips):
            q = lax.rem(y + dy, chips)
            se[dy, at] = (pe[ahead(dy), at].astype(f32) + re[q, at].astype(f32)).astype(bf16)
            exp_sum(i, dy).start()

    loop(n_group, push)

    total = pm[t].astype(f32) + rm[y].astype(f32)
    for dy in range(1, chips):
        mix_sum(dy).wait_recv()
        total = total + ym[dy].astype(f32)
    mo_ref[...] = total.astype(bf16)

    def finish(i):
        at = span_out(i)
        whole = pe[t, at].astype(f32) + re[y, at].astype(f32)
        for dy in range(1, chips):
            exp_sum(i, dy).wait_recv()
            whole = whole + yr[dy, at].astype(f32)
        fin[at] = whole.astype(bf16)
        first = lax.rem(home + 1 + i, n_group) * group
        for j in range(group):
            d = lax.rem(first + j - e + n_ep, n_ep)

            @pl.when(d != 0)
            def _():
                back(d).start()

    loop(n_group, finish)
    ret[e] = fin[e]
    loop(n_ep - 1, lambda d: back(d + 1).wait_recv())

    scores = rw_ref[...]
    normalized = scores / jnp.sum(scores, axis=1, keepdims=True) * routed_scale
    results = ret[...].reshape(slots, feat)
    eo_ref[...] = (
        normalized[:, 0:1] * jnp.dot(tables[0], results, preferred_element_type=f32)
        + normalized[:, 1:2] * jnp.dot(tables[1], results, preferred_element_type=f32)
    ).astype(bf16)

    def drain(d):
        dispatch(d + 1).wait_send()
        back(d + 1).wait_send()

    loop(n_ep - 1, drain)
    mix_p().wait_send()
    edge_copy().wait_send()
    for dy in range(1, chips):
        mix_y(dy).wait_send()
        mix_f(dy).wait_send()
        mix_sum(dy).wait_send()
    for q in range(chips):
        mix_half(q).wait_send()
        exp_half(q).wait_send()

    def drain_groups(i):
        exp_p(i).wait_send()
        for dy in range(1, chips):
            exp_y(i, dy).wait_send()
            exp_f(i, dy).wait_send()
            exp_sum(i, dy).wait_send()

    loop(n_group, drain_groups)


def solution(mesh):
    n_ep, n_tp = mesh.shape["ep"], mesh.shape["tp"]
    chips = n_tp // 2

    def local(
        mix_input, mix_gain, gate_b, gate_c, value_w, conv_weight, out_weight,
        expert_input, expert_gain, routes, route_weight, expert_gate, expert_up, expert_down,
    ):
        rows, feat = mix_input.shape
        width = feat * n_tp
        tok, top = routes.shape
        experts = n_ep * expert_gate.shape[0]
        assert expert_gate.shape[0] == 1 and top == 2
        cap = -(-(2 * tok * top // experts) // 16) * 16
        hidden = expert_gate.shape[2]
        group = max(1, n_ep // 8)
        n_group = n_ep // group
        slots = n_ep * cap
        vm, sem = pltpu.VMEM, pltpu.SemaphoreType.DMA
        scratch = [
            vm((width, feat), bf16), vm((width, feat), bf16), vm((width, feat), bf16),
            vm((feat, width), bf16),
            vm((1, width, hidden), bf16), vm((1, width, hidden), bf16), vm((hidden, width), bf16),
            sem((7,)),
            vm((2, tok, slots), bf16), vm((n_ep, cap, feat), bf16),
            vm((rows, width), bf16), vm((rows, width), bf16), vm((rows, 1), f32),
            vm((rows, feat), f32), vm((rows + 8, feat), f32), vm((8, feat), f32),
            vm((rows, feat), bf16),
            vm((n_tp, rows, feat), bf16), vm((chips, rows, feat), bf16),
            vm((chips, rows, feat), bf16), vm((chips, rows, feat), bf16),
            vm((n_ep, cap, width), bf16), vm((slots, width), bf16), vm((slots, 1), f32),
            vm((slots, hidden), bf16),
            vm((n_tp, n_ep, cap, feat), bf16), vm((chips, n_ep, cap, feat), bf16),
            vm((chips, n_ep, cap, feat), bf16), vm((chips, n_ep, cap, feat), bf16),
            vm((n_ep, cap, feat), bf16), vm((n_ep, cap, feat), bf16),
            sem((chips,)), sem((chips,)), sem((chips,)), sem((chips,)),
            sem((n_ep,)), sem((n_ep,)),
            sem((chips, n_group)), sem((chips, n_group)),
            sem((chips, n_group)), sem((chips, n_group)),
            sem((2,)),
            sem((chips,)), sem((chips,)), sem((chips,)), sem((chips,)),
            sem((chips,)), sem((chips,)),
            sem((chips, n_group)), sem((chips, n_group)),
            sem((n_ep,)), sem((n_ep,)),
        ]
        v = pl.BlockSpec(memory_space=pltpu.VMEM)
        a = pl.BlockSpec(memory_space=pl.ANY)
        return pl.pallas_call(
            functools.partial(kernel, (n_ep, n_tp, cap, group)),
            out_shape=(
                jax.ShapeDtypeStruct((rows, feat), bf16),
                jax.ShapeDtypeStruct((tok, feat), bf16),
            ),
            in_specs=[v, v, a, a, a, v, a, v, v, v, v, a, a, a],
            out_specs=(v, v),
            scratch_shapes=scratch,
            compiler_params=pltpu.CompilerParams(
                collective_id=0, has_side_effects=True, vmem_limit_bytes=62 << 20
            ),
        )(
            mix_input, mix_gain.reshape(1, -1), gate_b, gate_c, value_w, conv_weight, out_weight,
            expert_input, expert_gain.reshape(1, -1), routes, route_weight,
            expert_gate, expert_up, expert_down.reshape(hidden, width),
        )

    in_specs = (
        P("ep", "tp"), P(), P(None, "tp"), P(None, "tp"), P(None, "tp"), P(None, "tp"),
        P("tp", None), P("ep", "tp"), P(), P("ep", None), P("ep", None),
        P("ep", None, "tp"), P("ep", None, "tp"), P("ep", "tp", None),
    )
    out_specs = (P("ep", "tp"), P("ep", "tp"))
    return jax.shard_map(local, mesh=mesh, in_specs=in_specs, out_specs=out_specs, check_vma=False)
```

time: 158 us -> 76.8 us (0.49)
  waiting for transfers between devices: 70.1 us -> 0 us
  Pallas kernels: 0 us -> 69.6 us
  matrix products: 30.3 us -> 0 us
  blocking collectives: 24.9 us -> 0 us
  between operations: 13.9 us -> 0.64 us
  starting transfers between devices: 9.05 us -> 0 us
  other arithmetic: 5.51 us -> 0 us
  local copies, waits for them, and re-layouts: 4.3 us -> 6.22 us
    pallas_call x0 -> x1, Pallas kernels: none -> 69.6 us  [local(): pl.pallas_call(functools.partial(kernel, (n_ep, n_tp, cap, group)), out_s...]
    dot_general x7 -> x0, matrix products: 30.3 us -> none  [the longest x1 9.98 us: local(): jnp.einsum('gsf,gfd->dgs', activated, sliced, preferred_element_type=jnp....]
    all_gather x2 -> x0, waiting for transfers between devices: 26.8 us -> none  [the longest x1 23.6 us: local(): lax.all_gather(arrived, 'tp', axis=1, tiled=True)]
    reduce_scatter x2 -> x0, waiting for transfers between devices: 25.3 us -> none  [the longest x1 19.4 us: local(): lax.psum_scatter(summed.reshape(lax.axis_size('tp') * feature_local, loca...]
    all_to_all x1 -> x0, blocking collectives: 24.9 us -> none  [local(): lax.all_to_all(outgoing, 'ep', split_axis=0, concat_axis=2, tiled=True)]
    all_to_all x1 -> x0, waiting for transfers between devices: 16 us -> none  [local(): lax.all_to_all(returning, 'ep', split_axis=2, concat_axis=2, tiled=True)]
    all_to_all x1 -> x0, starting transfers between devices: 5.51 us -> none  [local(): lax.all_to_all(returning, 'ep', split_axis=2, concat_axis=2, tiled=True)]
    unnamed x19 -> x4, local copies, waits for them, and re-layouts: 1.01 us -> 6.22 us
  transfers between devices with their start and end apart: 6 -> 0, of which waited for: 6 -> 0; matrix products, arithmetic and copies ran while one was open for 22% -> 0% of each run, Pallas kernels for 0% -> 0%
where the time goes in v1:
time: 76.8 us; the launch traced here: 76.4 us
  Pallas kernels  69.6 us (91%)
  local copies, waits for them, and re-layouts  6.22 us (8%)
    pallas_call x1, Pallas kernels, local(): pl.pallas_call(functools.partial(kernel, (n_ep, n_tp, cap, group)), out_s...  69.6 us
    unnamed x4, local copies, waits for them, and re-layouts  6.22 us

profile of v1, /device:TPU:0, one launch (start us, length us, event | category | flops | bytes accessed | tf_op | source)
XLA Modules:
  0.0 76.4 jit_solution(10851694592678634105)
XLA Ops:
  0.6 1.4 %copy.16.routes_ref = s32[160,2]{1,0:T(8,128)} copy(s32[160,2]{0,1:T(2,128)} %param.23) | data formatting | bytes 2560 | tf_op args[9]
  2.1 1.4 %copy.17.rw_ref = f32[160,2]{1,0:T(8,128)} copy(f32[160,2]{0,1:T(2,128)} %param.24) | data formatting | bytes 2560 | tf_op args[10]
  3.5 69.6 %shard_map.149 = (bf16[384,512]{1,0:T(8,128)(2,1)}, bf16[160,512]{1,0:T(8,128)(2,1)}) custom-call(bf16[384,512]{1,0:T(8,128)(2,1)} %mix_ref.1, f32[1,2048]{1,0:T(1,128)} %bitcast.4, bf16[2048,512]{1,0:T(8,128)(2,1)} %wb_hbm.1, bf16[2048,512]{1,0:T(8,128)(2,1)} %wc_hbm.1, bf16[2048,512]{1,0:T(8,128)(2,1)} %wv_hbm.1, f32[3,512]{1,0:T(4,128)} %conv_ref.1, ...), custom_call_target="tpu_custom_call" | custom-call | tf_op jit(solution)/shard_map/pallas_call | solution.py:416
  73.1 1.8 %copy.20 = bf16[384,512]{1,0:T(8,128)(2,1)} copy(bf16[384,512]{1,0:T(8,128)(2,1)} %get-tuple-element.4) | data formatting | bytes 786432
  74.8 1.6 %copy.21 = bf16[160,512]{1,0:T(8,128)(2,1)} copy(bf16[160,512]{1,0:T(8,128)(2,1)} %get-tuple-element.5) | data formatting | bytes 327680

commit v2 on v1

--- a/solution.py
+++ b/solution.py
@@ -32,6 +32,7 @@
     width = feat * n_tp
     tok = exp_ref.shape[0]
     slots = n_ep * cap
+    half = n_ep // 2
     e = lax.axis_index("ep")
     t = lax.axis_index("tp")
     y, c = lax.div(t, 2), lax.rem(t, 2)
@@ -53,8 +54,8 @@
     def behind(dy):
         return lax.rem(y - dy + chips, chips) * 2 + c
 
-    def loop(count, body):
-        lax.fori_loop(0, count, lambda i, carry: (body(i), carry)[1], 0)
+    def loop(count, body, start=0):
+        lax.fori_loop(start, count, lambda i, carry: (body(i), carry)[1], 0)
 
     def mix_y(dy):
         return remote(mix_ref, xg.at[:, cols(t)], mys.at[dy], myr.at[dy], e, ahead(dy))
@@ -96,11 +97,21 @@
     def mix_sum(dy):
         return remote(sm.at[dy], ym.at[dy], yms.at[dy], ymr.at[dy], e, ahead(dy))
 
-    def exp_half(q):
-        return remote(pe.at[q * 2 + 1 - c], re.at[q], res.at[q], rer.at[q], e, partner)
+    def exp_half(q, h):
+        at = pl.ds(h * half, half)
+        return remote(
+            pe.at[q * 2 + 1 - c, at], re.at[q, at], res.at[h, q], rer.at[h, q], e, partner
+        )
 
     def span_out(i):
-        return pl.ds(lax.rem(home + 1 + i, n_group) * group, group)
+        return pl.ds(i * group, group)
+
+    def source(p):
+        return lax.rem(home - lax.div(p, group) + n_group, n_group) * group + lax.rem(p, group)
+
+    def place(s):
+        turn = lax.rem(home - lax.div(s, group) + n_group, n_group)
+        return turn * group + lax.rem(s, group)
 
     def exp_sum(i, dy):
         return remote(
@@ -110,7 +121,7 @@
 
     def back(d):
         s = lax.rem(e + d, n_ep)
-        return remote(fin.at[s], ret.at[e], rts.at[d], rtr.at[d], s, t)
+        return remote(fin.at[place(s)], ret.at[e], rts.at[d], rtr.at[d], s, t)
 
     loads = [
         pltpu.make_async_copy(src, dst, w_sem.at[i])
@@ -134,13 +145,17 @@
 
     loop(n_ep - 1, greet)
 
-    lane = lax.broadcasted_iota(jnp.int32, (tok, 128), 1)
-    named = [routes_ref[:, k : k + 1] == lane for k in range(2)]
+    row = lax.broadcasted_iota(jnp.int32, (tok, tok), 0)
+    column = lax.broadcasted_iota(jnp.int32, (tok, tok), 1)
+
+    def upright(line):
+        return jnp.sum(jnp.where(row == column, line, 0.0), axis=1, keepdims=True)
+
+    lane = lax.broadcasted_iota(jnp.int32, (tok, 128), 1).astype(f32)
+    chosen = [upright(routes_ref[k : k + 1, :].astype(f32)) for k in range(2)]
+    named = [chosen[k] == lane for k in range(2)]
     either = jnp.where(named[0] | named[1], 1.0, 0.0).astype(bf16)
-    before = (
-        lax.broadcasted_iota(jnp.int32, (tok, tok), 0)
-        > lax.broadcasted_iota(jnp.int32, (tok, tok), 1)
-    )
+    before = row > column
     counts = jnp.dot(
         jnp.where(before, 1.0, 0.0).astype(bf16), either, preferred_element_type=f32
     )
@@ -148,7 +163,7 @@
     both = []
     for k in range(2):
         rank = jnp.sum(jnp.where(named[k], counts, 0.0), axis=1, keepdims=True)
-        slot = routes_ref[:, k : k + 1].astype(f32) * float(cap) + rank
+        slot = chosen[k] * float(cap) + rank
         one = jnp.where(slot_iota == slot, 1.0, 0.0)
         tables[k] = one.astype(bf16)
         both.append(one)
@@ -183,7 +198,8 @@
             exp_y(i, dy).start()
         exp_p(i).start()
 
-    loop(n_group, pass_on)
+    early = n_group * 5 // 8
+    loop(early, pass_on)
 
     for dy in range(1, chips):
         mix_y(dy).wait_recv()
@@ -216,6 +232,75 @@
 
     loop(feat // wide, project)
     edge_copy().start()
+    loop(n_group, pass_on, early)
+
+    def relay(i):
+        for dy in range(1, chips):
+            exp_y(i, dy).wait_recv()
+            exp_f(i, dy).start()
+
+    def arrive(i):
+        exp_p(i).wait_recv()
+        for dy in range(1, chips):
+            exp_f(i, dy).wait_recv()
+
+    def scale_exp(p):
+        at = pl.ds(pl.multiple_of(p * cap, cap), cap)
+        x = xe[source(p)].astype(f32)
+        efac[at] = lax.rsqrt(jnp.sum(x * x, axis=1, keepdims=True) / width + epsilon)
+        xes[at] = (x * egain_ref[...]).astype(bf16)
+
+    hidden = wd.shape[0]
+    wide_h = 256 if hidden % 256 == 0 else hidden
+
+    def push(i):
+        at = span_out(i)
+        for dy in range(1, chips):
+            q = lax.rem(y + dy, chips)
+            se[dy, at] = (pe[ahead(dy), at].astype(f32) + re[q, at].astype(f32)).astype(bf16)
+            exp_sum(i, dy).start()
+
+    for h in range(2):
+        first, last = h * n_group // 2, (h + 1) * n_group // 2
+        loop(last, relay, first)
+        loop(last, arrive, first)
+        loop((h + 1) * half, scale_exp, h * half)
+        if h == 0:
+            loads[4].wait()
+            loads[5].wait()
+        part = pl.ds(h * half * cap, half * cap)
+
+        def activate(at):
+            x = xes[part]
+            factor = efac[part]
+            gate = jnp.dot(x, wg[0, :, at], preferred_element_type=f32) * factor
+            up = jnp.dot(x, wu[0, :, at], preferred_element_type=f32) * factor
+            act[part, at] = (gate / (1.0 + jnp.exp(-gate)) * up).astype(bf16)
+
+        if wide_h == hidden:
+            activate(slice(None))
+        else:
+            loop(
+                hidden // wide_h,
+                lambda i: activate(pl.ds(pl.multiple_of(i * wide_h, wide_h), wide_h)),
+            )
+        if h == 0:
+            loads[6].wait()
+
+        def exp_down(b):
+            out = jnp.dot(act[part], wd[:, cols(b)], preferred_element_type=f32)
+            pe[b, pl.ds(h * half, half)] = out.astype(bf16).reshape(half, cap, feat)
+
+        def exp_given(q):
+            exp_down(q * 2 + 1 - c)
+            exp_half(q, h).start()
+
+        loop(chips, exp_given)
+        loop(chips, lambda q: exp_down(q * 2 + c))
+        for q in range(chips):
+            exp_half(q, h).wait_recv()
+        loop(last, push, first)
+
     edge_copy().wait_recv()
     prod[0:8] = jnp.where(e == 0, 0.0, edge[...])
 
@@ -234,112 +319,52 @@
     def mix_down(b):
         pm[b] = jnp.dot(gated[...], wo[:, cols(b)], preferred_element_type=f32).astype(bf16)
 
-    loop(n_tp, mix_down)
-    for q in range(chips):
+    def mix_given(q):
+        mix_down(q * 2 + 1 - c)
         mix_half(q).start()
 
-    def relay(i):
-        for dy in range(1, chips):
-            exp_y(i, dy).wait_recv()
-            exp_f(i, dy).start()
-
+    loop(chips, mix_given)
+    loop(chips, lambda q: mix_down(q * 2 + c))
     for q in range(chips):
         mix_half(q).wait_recv()
     for dy in range(1, chips):
         q = lax.rem(y + dy, chips)
         sm[dy] = (pm[ahead(dy)].astype(f32) + rm[q].astype(f32)).astype(bf16)
         mix_sum(dy).start()
-    loop(n_group, relay)
-
-    def arrive(i):
-        exp_p(i).wait_recv()
-        for dy in range(1, chips):
-            exp_f(i, dy).wait_recv()
-
-    loop(n_group, arrive)
-
-    def scale_exp(i):
-        at = pl.ds(pl.multiple_of(i * cap, cap), cap)
-        x = xe[i].astype(f32)
-        efac[at] = lax.rsqrt(jnp.sum(x * x, axis=1, keepdims=True) / width + epsilon)
-        xes[at] = (x * egain_ref[...]).astype(bf16)
-
-    loop(n_ep, scale_exp)
-    loads[4].wait()
-    loads[5].wait()
-    hidden = wd.shape[0]
-    wide_h = 256 if hidden % 256 == 0 else hidden
-
-    def activate(i):
-        at = pl.ds(i * wide_h, wide_h) if wide_h == hidden else pl.ds(
-            pl.multiple_of(i * wide_h, wide_h), wide_h
-        )
-        x = xes[...]
-        gate = jnp.dot(x, wg[0, :, at], preferred_element_type=f32) * efac[...]
-        up = jnp.dot(x, wu[0, :, at], preferred_element_type=f32) * efac[...]
-        act[:, at] = (gate / (1.0 + jnp.exp(-gate)) * up).astype(bf16)
-
-    if wide_h == hidden:
-        x = xes[...]
-        gate = jnp.dot(x, wg[0], preferred_element_type=f32) * efac[...]
-        up = jnp.dot(x, wu[0], preferred_element_type=f32) * efac[...]
-        act[...] = (gate / (1.0 + jnp.exp(-gate)) * up).astype(bf16)
-    else:
-        loop(hidden // wide_h, activate)
-    loads[6].wait()
-
-    def exp_down(b):
-        out = jnp.dot(act[...], wd[:, cols(b)], preferred_element_type=f32)
-        pe[b] = out.astype(bf16).reshape(n_ep, cap, feat)
-
-    loop(n_tp, exp_down)
-    for q in range(chips):
-        exp_half(q).start()
-
-    for q in range(chips):
-        exp_half(q).wait_recv()
-
-    def push(i):
+
+    def finish(i):
         at = span_out(i)
-        for dy in range(1, chips):
-            q = lax.rem(y + dy, chips)
-            se[dy, at] = (pe[ahead(dy), at].astype(f32) + re[q, at].astype(f32)).astype(bf16)
-            exp_sum(i, dy).start()
-
-    loop(n_group, push)
+        whole = pe[t, at].astype(f32) + re[y, at].astype(f32)
+        for dy in range(1, chips):
+            exp_sum(i, dy).wait_recv()
+            whole = whole + yr[dy, at].astype(f32)
+        fin[at] = whole.astype(bf16)
+        first = lax.rem(home - i + n_group, n_group) * group
+        for j in range(group):
+            d = lax.rem(first + j - e + n_ep, n_ep)
+
+            @pl.when(d != 0)
+            def _():
+                back(d).start()
+
+    loop(n_group, finish)
+    ret[e] = fin[place(e)]
+    loop(n_ep - 1, lambda d: back(d + 1).wait_recv())
+
+    scores = rw_ref[...]
+    normalized = scores / jnp.sum(scores, axis=0, keepdims=True) * routed_scale
+    share = [upright(normalized[k : k + 1, :]) for k in range(2)]
+    results = ret[...].reshape(slots, feat)
+    eo_ref[...] = (
+        share[0] * jnp.dot(tables[0], results, preferred_element_type=f32)
+        + share[1] * jnp.dot(tables[1], results, preferred_element_type=f32)
+    ).astype(bf16)
 
     total = pm[t].astype(f32) + rm[y].astype(f32)
     for dy in range(1, chips):
         mix_sum(dy).wait_recv()
         total = total + ym[dy].astype(f32)
     mo_ref[...] = total.astype(bf16)
-
-    def finish(i):
-        at = span_out(i)
-        whole = pe[t, at].astype(f32) + re[y, at].astype(f32)
-        for dy in range(1, chips):
-            exp_sum(i, dy).wait_recv()
-            whole = whole + yr[dy, at].astype(f32)
-        fin[at] = whole.astype(bf16)
-        first = lax.rem(home + 1 + i, n_group) * group
-        for j in range(group):
-            d = lax.rem(first + j - e + n_ep, n_ep)
-
-            @pl.when(d != 0)
-            def _():
-                back(d).start()
-
-    loop(n_group, finish)
-    ret[e] = fin[e]
-    loop(n_ep - 1, lambda d: back(d + 1).wait_recv())
-
-    scores = rw_ref[...]
-    normalized = scores / jnp.sum(scores, axis=1, keepdims=True) * routed_scale
-    results = ret[...].reshape(slots, feat)
-    eo_ref[...] = (
-        normalized[:, 0:1] * jnp.dot(tables[0], results, preferred_element_type=f32)
-        + normalized[:, 1:2] * jnp.dot(tables[1], results, preferred_element_type=f32)
-    ).astype(bf16)
 
     def drain(d):
         dispatch(d + 1).wait_send()
@@ -354,7 +379,8 @@
         mix_sum(dy).wait_send()
     for q in range(chips):
         mix_half(q).wait_send()
-        exp_half(q).wait_send()
+        exp_half(q, 0).wait_send()
+        exp_half(q, 1).wait_send()
 
     def drain_groups(i):
         exp_p(i).wait_send()
@@ -407,7 +433,7 @@
             sem((chips, n_group)), sem((chips, n_group)),
             sem((2,)),
             sem((chips,)), sem((chips,)), sem((chips,)), sem((chips,)),
-            sem((chips,)), sem((chips,)),
+            sem((2, chips)), sem((2, chips)),
             sem((chips, n_group)), sem((chips, n_group)),
             sem((n_ep,)), sem((n_ep,)),
         ]
@@ -427,7 +453,7 @@
             ),
         )(
             mix_input, mix_gain.reshape(1, -1), gate_b, gate_c, value_w, conv_weight, out_weight,
-            expert_input, expert_gain.reshape(1, -1), routes, route_weight,
+            expert_input, expert_gain.reshape(1, -1), routes.T, route_weight.T,
             expert_gate, expert_up, expert_down.reshape(hidden, width),
         )
 

time: 76.8 us -> 67.7 us (0.88)
  Pallas kernels: 69.6 us -> 63.5 us
  local copies, waits for them, and re-layouts: 6.22 us -> 3.36 us
    pallas_call x1, Pallas kernels: 69.6 us -> 63.5 us  [local(): pl.pallas_call(functools.partial(kernel, (n_ep, n_tp, cap, group)), out_s...]
    unnamed x4 -> x2, local copies, waits for them, and re-layouts: 6.22 us -> 3.36 us
where the time goes in v2:
time: 67.7 us; the launch traced here: 67.5 us
  Pallas kernels  63.5 us (94%)
  local copies, waits for them, and re-layouts  3.36 us (5%)
    pallas_call x1, Pallas kernels, local(): pl.pallas_call(functools.partial(kernel, (n_ep, n_tp, cap, group)), out_s...  63.5 us
    unnamed x2, local copies, waits for them, and re-layouts  3.36 us

profile of v2, /device:TPU:0, one launch (start us, length us, event | category | flops | bytes accessed | tf_op | source)
XLA Modules:
  0.0 67.5 jit_solution(9519356107450748406)
XLA Ops:
  0.6 63.5 %shard_map.149 = (bf16[384,512]{1,0:T(8,128)(2,1)}, bf16[160,512]{1,0:T(8,128)(2,1)}) custom-call(bf16[384,512]{1,0:T(8,128)(2,1)} %mix_ref.1, f32[1,2048]{1,0:T(1,128)} %bitcast.6, bf16[2048,512]{1,0:T(8,128)(2,1)} %wb_hbm.1, bf16[2048,512]{1,0:T(8,128)(2,1)} %wc_hbm.1, bf16[2048,512]{1,0:T(8,128)(2,1)} %wv_hbm.1, f32[3,512]{1,0:T(4,128)} %conv_ref.1, ...), custom_call_target="tpu_custom_call" | custom-call | tf_op jit(solution)/shard_map/pallas_call | solution.py:442
  64.2 1.8 %copy.18 = bf16[384,512]{1,0:T(8,128)(2,1)} copy(bf16[384,512]{1,0:T(8,128)(2,1)} %get-tuple-element.4) | data formatting | bytes 786432
  65.9 1.6 %copy.19 = bf16[160,512]{1,0:T(8,128)(2,1)} copy(bf16[160,512]{1,0:T(8,128)(2,1)} %get-tuple-element.5) | data formatting | bytes 327680
